TPU v7x, 32 devices: a whole 2x2x4 slice. The times are simulated.
32 devices in a mesh: ep: 8 (over z, x), tp: 4 (over y, core).
Axes of the slice: x: 2, y: 2, z: 4, core: 2. Of those that a mesh axis runs over, the one named last changes fastest.
Arguments:
- tokens: bfloat16 [128, 4096], P('ep'), may hold values from -6 to 6
- norm_gain: float32 [4096], replicated, may hold values from 0.1 to 1.9
- query_weight: bfloat16 [4096, 2048], P('ep', 'tp'), may hold values from -0.09375 to 0.09375
- key_weight: bfloat16 [4096, 256], P('ep', 'tp'), may hold values from -0.09375 to 0.09375
- value_weight: bfloat16 [4096, 256], P('ep', 'tp'), may hold values from -0.09375 to 0.09375
- forget_weight: bfloat16 [4096, 32], P('ep', 'tp'), may hold values from -0.09375 to 0.09375
- forget_bias: float32 [32], P('tp'), may hold values from -1 to 2
- kv_cache: bfloat16 [128, 1024, 4, 128], P('ep', None, 'tp'), may hold values from -256 to 256, as said below
- log_gates: float32 [128, 1024, 32], P('ep', None, 'tp'), may hold values from -258 to 0
- lengths: int32 [128], P('ep'), may hold values from 128 to 1024, as said below
- out_weight: bfloat16 [2048, 4096], P('tp', 'ep'), may hold values from -0.125 to 0.125
- mix_gain: float32 [4096], replicated, may hold values from 0.1 to 1.9
- expert_gate: bfloat16 [8, 4096, 1024], P('ep', None, 'tp'), may hold values from -0.09375 to 0.09375
- expert_up: bfloat16 [8, 4096, 1024], P('ep', None, 'tp'), may hold values from -0.09375 to 0.09375
- expert_down: bfloat16 [8, 1024, 4096], P('ep', 'tp'), may hold values from -0.1875 to 0.1875
- routes: int32 [128, 4], P('ep'), may hold values from 0 to 7, all different within a row; in each aligned block of 16 rows (0 to 15, 16 to 31, ...) at most 16 rows name the same one
- route_weights: float32 [128, 4], P('ep'), may hold values from 0.2 to 1
- dense_gate: bfloat16 [4096, 4096], P(None, 'ep'), may hold values from -0.09375 to 0.09375
- dense_up: bfloat16 [4096, 4096], P(None, 'ep'), may hold values from -0.09375 to 0.09375
- dense_down: bfloat16 [4096, 4096], P('ep', 'tp'), may hold values from -0.09375 to 0.09375
- gate_vector: float32 [4096], replicated, may hold values from -0.09375 to 0.09375
Outputs:
- layer_out: bfloat16 [128, 4096], P('ep', 'tp')
Inputs may be any that keep to these rules, and one draw needn't show every extreme that they name: `kv_cache`: keys and values of the cached positions. `lengths`: some sequence uses all 1024 cached positions in every draw. A sequence's 4 experts differ. Among the routes of the 16 sequences of one index of ep no expert appears more than 16 times, and in every draw some expert appears exactly 16 times there; every expert is chosen somewhere.
All inputs are finite; a program needn't handle non-finite values.
Results may differ from a plain program's by a relative error of at most 0.012.
The roundings to bfloat16 on the way count: a program that leaves them out, or rounds other values in their place, can miss the bound.
Values may be sent and summed in bfloat16 or wider, within the bound.
No kernel may reach another device: no remote copies, remote signals or barrier semaphores. Data moves between devices by JAX's collectives and lax.ppermute only.
A program may use at most 128 MiB of HBM per device.

v0:
```python
import jax
import jax.numpy as jnp
from jax import lax
from jax.sharding import PartitionSpec as P

EPS = 1e-06


def rms_scaled(matrix, gains):
    values = matrix.astype(jnp.float32)
    return values * lax.rsqrt(jnp.mean(values * values, axis=-1, keepdims=True) + EPS) * gains


def attend_local(queries, key_new, value_new, forget, kv_cache, log_gates, lengths):
    seqs_here, cache_len, kv_count, double_width = kv_cache.shape
    head_width = double_width // 2
    group_size = queries.shape[1] // (kv_count * head_width)
    queries = queries.reshape(seqs_here, kv_count, group_size, head_width)
    key_new = key_new.reshape(seqs_here, kv_count, head_width)
    value_new = value_new.reshape(seqs_here, kv_count, head_width)
    cached_keys = kv_cache[..., :head_width]
    cached_values = kv_cache[..., head_width:]
    score_scale = head_width ** (-0.5)
    current_position = jnp.arange(cache_len, dtype=jnp.int32)
    is_last = (current_position[None, :] == lengths[:, None] - 1)[:, :, None]
    last_gate = jnp.sum(jnp.where(is_last, log_gates, 0.0), axis=1)
    newest = last_gate + forget
    gate_bias = newest[:, None, :] - log_gates
    gate_bias = gate_bias.reshape(seqs_here, cache_len, kv_count, group_size).transpose(0, 2, 3, 1)
    past_scores = (
        jnp.einsum("skgd,slkd->skgl", queries, cached_keys, preferred_element_type=jnp.float32)
        * score_scale
        + gate_bias
    )
    is_valid = (current_position[None, :] < lengths[:, None])[:, None, None, :]
    past_scores = jnp.where(is_valid, past_scores, -jnp.inf)
    own_score = (
        jnp.einsum("skgd,skd->skg", queries, key_new, preferred_element_type=jnp.float32)
        * score_scale
    )
    highest = jnp.maximum(jnp.max(past_scores, axis=-1), own_score)
    past_exp = jnp.exp(past_scores - highest[..., None])
    own_exp = jnp.exp(own_score - highest)
    totals = jnp.sum(past_exp, axis=-1) + own_exp
    past_weights = (past_exp / totals[..., None]).astype(jnp.bfloat16)
    own_weights = (own_exp / totals).astype(jnp.bfloat16)
    mixed_values = jnp.einsum(
        "skgl,slkd->skgd", past_weights, cached_values, preferred_element_type=jnp.float32
    )
    mixed_values = (
        mixed_values
        + own_weights.astype(jnp.float32)[..., None] * value_new.astype(jnp.float32)[:, :, None, :]
    )
    return mixed_values.astype(jnp.bfloat16).reshape(seqs_here, kv_count * group_size * head_width)


def shards(
    tokens,
    norm_gain,
    query_weight,
    key_weight,
    value_weight,
    forget_weight,
    forget_bias,
    kv_cache,
    log_gates,
    lengths,
    out_weight,
    mix_gain,
    expert_gate,
    expert_up,
    expert_down,
    routes,
    route_weights,
    dense_gate,
    dense_up,
    dense_down,
    gate_vector,
):
    seq_count = tokens.shape[0]
    normed = rms_scaled(tokens, norm_gain).astype(jnp.bfloat16)
    query_cols = query_weight.shape[1]
    key_cols = key_weight.shape[1]
    columns = lax.all_to_all(normed, "ep", split_axis=1, concat_axis=0, tiled=True)
    row_block = columns
    projected = lax.psum_scatter(
        jnp.concatenate(
            [
                jnp.dot(row_block, matrix, preferred_element_type=jnp.float32)
                for matrix in (query_weight, key_weight, value_weight, forget_weight)
            ],
            axis=1,
        ),
        "ep",
        scatter_dimension=0,
        tiled=True,
    )
    queries = projected[:, :query_cols].astype(jnp.bfloat16)
    key_new = projected[:, query_cols : query_cols + key_cols].astype(jnp.bfloat16)
    value_new = projected[:, query_cols + key_cols : query_cols + 2 * key_cols].astype(jnp.bfloat16)
    forget = jax.nn.log_sigmoid(projected[:, query_cols + 2 * key_cols :] + forget_bias)
    attended = attend_local(queries, key_new, value_new, forget, kv_cache, log_gates, lengths)
    column_terms = jnp.dot(
        lax.all_gather(attended, "ep", axis=0, tiled=True),
        out_weight,
        preferred_element_type=jnp.float32,
    )
    column_total = lax.psum(column_terms, "tp")
    summed = lax.all_to_all(column_total, "ep", split_axis=0, concat_axis=1, tiled=True)
    mixed = (tokens.astype(jnp.float32) + summed).astype(jnp.bfloat16)
    second = rms_scaled(mixed, mix_gain).astype(jnp.bfloat16)
    gate_value = jax.nn.sigmoid(
        jnp.dot(second.astype(jnp.float32), gate_vector, precision=lax.Precision.HIGHEST)
    )
    experts = lax.axis_size("ep")
    top_count = routes.shape[1]
    capacity = max(2, 2 * seq_count * top_count // experts)
    flat_routes = routes.reshape(-1)
    one_hot = (flat_routes[:, None] == jnp.arange(experts, dtype=jnp.int32)[None, :]).astype(
        jnp.int32
    )
    earlier = jnp.sum((jnp.cumsum(one_hot, axis=0) - one_hot) * one_hot, axis=1)
    slot_index = (flat_routes * capacity + earlier).reshape(seq_count, top_count)
    slot_ids = jnp.arange(experts * capacity, dtype=jnp.int32)
    dispatch_map = jnp.any(slot_index[None, :, :] == slot_ids[:, None, None], axis=2).astype(
        jnp.bfloat16
    )
    outgoing = jnp.dot(dispatch_map, second, preferred_element_type=jnp.float32).astype(
        jnp.bfloat16
    )
    outgoing = outgoing.reshape(experts, capacity, second.shape[1])
    received = lax.all_to_all(outgoing, "ep", split_axis=0, concat_axis=0, tiled=True)
    sources, items, model_width = received.shape
    flat_rows = received.reshape(sources * items, model_width)
    gate_pre = jnp.dot(flat_rows, expert_gate[0], preferred_element_type=jnp.float32)
    up_pre = jnp.dot(flat_rows, expert_up[0], preferred_element_type=jnp.float32)
    hidden = (jax.nn.silu(gate_pre) * up_pre).astype(jnp.bfloat16)
    partial_rows = jnp.dot(hidden, expert_down[0], preferred_element_type=jnp.float32)
    reduced = lax.psum_scatter(partial_rows, "tp", scatter_dimension=1, tiled=True)
    replies = reduced.astype(jnp.bfloat16).reshape(sources, items, reduced.shape[1])
    returned = lax.all_to_all(replies, "ep", split_axis=0, concat_axis=0, tiled=True)
    quarter_cols = returned.shape[2]
    picked = returned.reshape(experts * capacity, quarter_cols)[slot_index.reshape(-1)]
    routed = jnp.sum(
        picked.astype(jnp.float32).reshape(seq_count, top_count, quarter_cols)
        * route_weights[:, :, None],
        axis=1,
    )
    tp_index = lax.axis_index("tp")
    piece = lax.all_gather(second, "ep", axis=0, tiled=True)
    dense_hidden = (
        jax.nn.silu(jnp.dot(piece, dense_gate, preferred_element_type=jnp.float32))
        * jnp.dot(piece, dense_up, preferred_element_type=jnp.float32)
    ).astype(jnp.bfloat16)
    row_block = dense_hidden
    dense_out = lax.psum_scatter(
        jnp.dot(row_block, dense_down, preferred_element_type=jnp.float32),
        "ep",
        scatter_dimension=0,
        tiled=True,
    )
    residual = lax.dynamic_slice_in_dim(mixed, tp_index * quarter_cols, quarter_cols, 1).astype(
        jnp.float32
    )
    return (residual + routed + gate_value[:, None] * dense_out).astype(jnp.bfloat16)


def solution(mesh):
    return jax.shard_map(
        shards,
        mesh=mesh,
        in_specs=(
            P("ep", None),
            P(),
            P("ep", "tp"),
            P("ep", "tp"),
            P("ep", "tp"),
            P("ep", "tp"),
            P("tp"),
            P("ep", None, "tp", None),
            P("ep", None, "tp"),
            P("ep"),
            P("tp", "ep"),
            P(),
            P("ep", None, "tp"),
            P("ep", None, "tp"),
            P("ep", "tp", None),
            P("ep", None),
            P("ep", None),
            P(None, "ep"),
            P(None, "ep"),
            P("ep", "tp"),
            P(),
        ),
        out_specs=P("ep", "tp"),
        check_vma=False,
    )
```

profile of v0, /device:TPU:0, one launch (start us, length us, event | category | flops | bytes accessed | tf_op | source)
XLA Modules:
  0.0 333.0 jit_solution(12179301577359732236)
XLA Ops:
  6.6 1.2 fusion.48
  7.8 1.0 fusion.50
  8.9 14.4 %all_to_all.48 = bf16[16,8,512]{2,0,1:T(8,128)(2,1)S(1)} all-to-all(bf16[16,8,512]{2,0,1:T(8,128)(2,1)S(1)} %bitcast.121), channel_id=1, replica_groups=mesh['ep'=8,'tp'=4] {'ep'}, dimensions={1} | all-to-all | bytes 262144 | tf_op jit(solution)/shard_map/all_to_all | solution.py:84
  23.3 0.8 fusion.84
  24.1 1.0 fusion.83
  25.2 1.0 fusion.82
  26.2 1.3 fusion.81
  27.5 0.9 pad_maximum_fusion
  29.4 59.1 %reduce-scatter.4.cloned.1.call-done = f32[16,648]{1,0:T(8,128)} async-done(((f32[128,648]{1,0:T(8,128)}), f32[16,648]{1,0:T(8,128)}) %reduce-scatter.4.cloned.1.call-update) | async-done | bytes 41488 | tf_op jit(solution)/shard_map/reduce_scatter | solution.py:86
  89.6 0.9 fusion.69
  90.5 3.7 %fusion.80 = (f32[16,8]{1,0:T(8,128)S(1)}, f32[16,1,8,1024]{3,2,0,1:T(8,128)S(1)}) fusion(f32[16,1024,8]{1,2,0:T(8,128)S(1)} %copy-done.3, f32[16,8]{1,0:T(8,128)S(1)} %fusion.69, bf16[16,8,64]{2,1,0:T(8,128)(2,1)S(1)} %reshape.186, bf16[16,1024,1,128]{3,1,2,0:T(8,128)(2,1)} %param.28, pred[16,1024]{1,0:T(8,128)(4,1)S(1)} %iota_compare_fusion.1), kind=kOutput, calls=%fused_computation.96 | convolution fusion | flops 17432448 | bytes 5276672 | tf_op jit(solution)/shard_map/skgd,slkd->skgl/dot_general | solution.py:31
  94.5 1.4 fusion.37
  96.0 30.5 %all_gather.6 = bf16[128,512]{1,0:T(8,128)(2,1)S(1)} all-gather(bf16[16,512]{1,0:T(8,128)(2,1)S(1)} %reshape.191), channel_id=1, replica_groups=mesh['ep'=8,'tp'=4] {'ep'}, dimensions={0}, use_global_device_ids=true | all-gather | bytes 147456 | tf_op jit(solution)/shard_map/all_gather | solution.py:104
  126.6 0.9 fusion.85
  127.7 31.3 %all-reduce.2.cloned.1.call-done = f32[8,16,512]{2,1,0:T(8,128)} async-done(((f32[8,16,512]{2,1,0:T(8,128)}), f32[8,16,512]{2,1,0:T(8,128)}) %all-reduce.2.cloned.1.call-update) | async-done | bytes 262160 | tf_op jit(solution)/shard_map/psum | solution.py:108
  159.0 5.5 %all-to-all-start.1 = ((f32[8,16,512]{2,1,0:T(8,128)}), f32[8,16,512]{2,1,0:T(8,128)S(1)}, u32[]{:S(2)}, u32[]{:S(2)}) async-start(f32[8,16,512]{2,1,0:T(8,128)} %all-reduce.2.cloned.1.call-done), calls=%async_computation.2 | async-start | bytes 524288 | tf_op jit(solution)/shard_map/all_to_all | solution.py:109
  165.2 7.6 %all-to-all-done.1 = f32[8,16,512]{2,1,0:T(8,128)S(1)} async-done(((f32[8,16,512]{2,1,0:T(8,128)}), f32[8,16,512]{2,1,0:T(8,128)S(1)}, u32[]{:S(2)}, u32[]{:S(2)}) %all-to-all-start.1) | async-done | bytes 262176 | tf_op jit(solution)/shard_map/all_to_all | solution.py:109
  173.1 1.5 convolution_convert_fusion
  174.6 3.6 %all-to-all-start.2 = ((bf16[8,16,4096]{2,1,0:T(8,128)(2,1)}), bf16[8,16,4096]{2,1,0:T(8,128)(2,1)S(1)}, u32[]{:S(2)}, u32[]{:S(2)}) async-start(bf16[8,16,4096]{2,1,0:T(8,128)(2,1)} %bitcast.112), calls=%async_computation.3 | async-start | bytes 2097152 | tf_op jit(solution)/shard_map/all_to_all | solution.py:132
  178.9 27.4 %all-to-all-done.2 = bf16[8,16,4096]{2,1,0:T(8,128)(2,1)S(1)} async-done(((bf16[8,16,4096]{2,1,0:T(8,128)(2,1)}), bf16[8,16,4096]{2,1,0:T(8,128)(2,1)S(1)}, u32[]{:S(2)}, u32[]{:S(2)}) %all-to-all-start.2) | async-done | bytes 1048608 | tf_op jit(solution)/shard_map/all_to_all | solution.py:132
  206.3 2.0 fusion.10
  208.4 4.3 %fusion.6 = f32[128,4096]{1,0:T(8,128)} fusion(bf16[1,256,4096]{2,1,0:T(8,128)(2,1)S(1)} %copy-done, bf16[128,4096]{1,0:T(8,128)(2,1)S(1)} %bitcast.110, bf16[1,4096,256]{2,1,0:T(8,128)(2,1)} %param.34, f32[128,256]{1,0:T(8,128)S(1)} %fusion.10), kind=kOutput, calls=%fused_computation.8 | convolution fusion | flops 537067520 | bytes 7471104 | tf_op jit(solution)/shard_map/dot_general | solution.py:138
  212.7 14.0 %all-gather.2.cloned.1.call-done = bf16[128,4096]{1,0:T(8,128)(2,1)} async-done(((bf16[16,4096]{1,0:T(8,128)(2,1)}), bf16[128,4096]{1,0:T(8,128)(2,1)}) %all-gather.2.cloned.1.call-update) | async-done | bytes 1048592 | tf_op jit(solution)/shard_map/all_gather | solution.py:150
  226.7 3.3 fusion.86
  230.1 4.3 %fusion.25 = f32[128,1024]{1,0:T(8,128)} fusion(bf16[512,1024]{1,0:T(8,128)(2,1)} %param.40, bf16[128,4096]{1,0:T(8,128)(2,1)S(1)} %copy-done.2, bf16[4096,512]{1,0:T(8,128)(2,1)} %param.39, f32[128,512]{1,0:T(8,128)S(1)} %fusion.86), kind=kOutput, calls=%fused_computation.20 | convolution fusion | flops 671481856 | bytes 7077888 | tf_op jit(solution)/shard_map/dot_general | solution.py:157
  234.6 24.5 %reduce-scatter.6.cloned.1.call-done = f32[128,1024]{1,0:T(8,128)} async-done(((f32[128,4096]{1,0:T(8,128)}), f32[128,1024]{1,0:T(8,128)}) %reduce-scatter.6.cloned.1.call-update) | async-done | bytes 524304 | tf_op jit(solution)/shard_map/reduce_scatter | solution.py:139
  259.0 1.8 convert_element_type.82
  260.8 5.5 %all-to-all-start.3 = ((bf16[8,16,1024]{2,1,0:T(8,128)(2,1)}), bf16[8,16,1024]{2,1,0:T(8,128)(2,1)S(1)}, u32[]{:S(2)}, u32[]{:S(2)}) async-start(bf16[8,16,1024]{2,1,0:T(8,128)(2,1)} %bitcast.19), calls=%async_computation.5 | async-start | bytes 524288 | tf_op jit(solution)/shard_map/all_to_all | solution.py:141
  266.4 0.9 fusion.43
  267.3 8.6 %all-to-all-done.3 = bf16[8,16,1024]{2,1,0:T(8,128)(2,1)S(1)} async-done(((bf16[8,16,1024]{2,1,0:T(8,128)(2,1)}), bf16[8,16,1024]{2,1,0:T(8,128)(2,1)S(1)}, u32[]{:S(2)}, u32[]{:S(2)}) %all-to-all-start.3) | async-done | bytes 262176 | tf_op jit(solution)/shard_map/all_to_all | solution.py:141
  276.9 48.0 %reduce-scatter.8.cloned.1.call-done = f32[16,1024]{1,0:T(8,128)} async-done(((f32[128,1024]{1,0:T(8,128)}), f32[16,1024]{1,0:T(8,128)}) %reduce-scatter.8.cloned.1.call-update) | async-done | bytes 65552 | tf_op jit(solution)/shard_map/reduce_scatter | solution.py:156
  324.9 1.5 add_convert_fusion
  (73 shorter events, 5.7 us)
Async XLA Ops:
  6.5 201.8 %copy-start = (bf16[1,256,4096]{2,1,0:T(8,128)(2,1)S(1)}, bf16[1,256,4096]{2,1,0:T(8,128)(2,1)}, u32[]{:S(2)}) copy-start(bf16[1,256,4096]{2,1,0:T(8,128)(2,1)} %param.35) | copy-start | bytes 6291460
  6.5 22.8 %copy-start.12 = (s32[16]{0:T(128)S(1)}, s32[16]{0:T(128)}, u32[]{:S(2)}) copy-start(s32[16]{0:T(128)} %param.30) | copy-start | bytes 196
  6.5 22.6 %copy-start.3 = (f32[16,1024,8]{1,2,0:T(8,128)S(1)}, f32[16,1024,8]{1,2,0:T(8,128)}, u32[]{:S(2)}) copy-start(f32[16,1024,8]{1,2,0:T(8,128)} %param.29) | copy-start | bytes 1572868
  6.5 83.1 %copy-start.13 = (f32[8]{0:T(128)S(1)}, f32[8]{0:T(128)}, u32[]{:S(2)}) copy-start(f32[8]{0:T(128)} %param.27) | copy-start | bytes 100
  6.5 82.0 %reduce-scatter.4.cloned.1.call-start = ((), (), s32[]{:S(2)}) async-start(), calls=%async_computation.7 | async-start | bytes 442368 | tf_op jit(solution)/shard_map/reduce_scatter | solution.py:86
  28.3 130.7 %all-reduce.2.cloned.1.call-start = ((), (), s32[]{:S(2)}) async-start(), calls=%async_computation.8 | async-start | bytes 524288 | tf_op jit(solution)/shard_map/psum | solution.py:108
  89.5 5.0 %copy-start.1 = (bf16[16,1024,1,128]{3,1,2,0:T(8,128)(2,1)S(1)}, bf16[16,1024,1,128]{3,1,2,0:T(8,128)(2,1)}, u32[]{:S(2)}) copy-start(bf16[16,1024,1,128]{3,1,2,0:T(8,128)(2,1)} %param.28) | copy-start | bytes 12582916
  94.2 32.3 %copy-start.8 = (bf16[512,512]{1,0:T(8,128)(2,1)S(1)}, bf16[512,512]{1,0:T(8,128)(2,1)}, u32[]{:S(2)}) copy-start(bf16[512,512]{1,0:T(8,128)(2,1)} %param.31) | copy-start | bytes 1572868
  94.2 33.3 %copy-start.10 = (s32[16,4]{0,1:T(4,128)S(1)}, s32[16,4]{0,1:T(4,128)}, u32[]{:S(2)}) copy-start(s32[16,4]{0,1:T(4,128)} %param.36) | copy-start | bytes 772
  94.5 78.3 %copy-start.4 = (bf16[16,4096]{1,0:T(8,128)(2,1)S(1)}, bf16[16,4096]{1,0:T(8,128)(2,1)}, u32[]{:S(2)}) copy-start(bf16[16,4096]{1,0:T(8,128)(2,1)} %param.21) | copy-start | bytes 393220
  94.5 78.5 %copy-start.9 = (f32[4096]{0:T(1024)S(1)}, f32[4096]{0:T(1024)}, u32[]{:S(2)}) copy-start(f32[4096]{0:T(1024)} %param.32) | copy-start | bytes 49156
  159.0 13.7 %all-to-all-start.1 = ((f32[8,16,512]{2,1,0:T(8,128)}), f32[8,16,512]{2,1,0:T(8,128)S(1)}, u32[]{:S(2)}, u32[]{:S(2)}) async-start(f32[8,16,512]{2,1,0:T(8,128)} %all-reduce.2.cloned.1.call-done), calls=%async_computation.2 | async-start | bytes 524288 | tf_op jit(solution)/shard_map/all_to_all | solution.py:109
  173.0 1.6 copy-start.7
  173.1 5.1 %copy-start.5 = (bf16[16,4096]{1,0:T(8,128)(2,1)}, bf16[16,4096]{1,0:T(8,128)(2,1)S(1)}, u32[]{:S(2)}) copy-start(bf16[16,4096]{1,0:T(8,128)(2,1)S(1)} %fusion.47) | copy-start | bytes 393220
  174.6 31.8 %all-to-all-start.2 = ((bf16[8,16,4096]{2,1,0:T(8,128)(2,1)}), bf16[8,16,4096]{2,1,0:T(8,128)(2,1)S(1)}, u32[]{:S(2)}, u32[]{:S(2)}) async-start(bf16[8,16,4096]{2,1,0:T(8,128)(2,1)} %bitcast.112), calls=%async_computation.3 | async-start | bytes 2097152 | tf_op jit(solution)/shard_map/all_to_all | solution.py:132
  178.1 48.6 %all-gather.2.cloned.1.call-start = ((), (), s32[]{:S(2)}) async-start(), calls=%async_computation.10 | async-start | bytes 1179648 | tf_op jit(solution)/shard_map/all_gather | solution.py:150
  178.9 80.2 %reduce-scatter.6.cloned.1.call-start = ((), (), s32[]{:S(2)}) async-start(), calls=%async_computation.9 | async-start | bytes 2621440 | tf_op jit(solution)/shard_map/reduce_scatter | solution.py:139
  212.7 112.2 %reduce-scatter.8.cloned.1.call-start = ((), (), s32[]{:S(2)}) async-start(), calls=%async_computation.11 | async-start | bytes 589824 | tf_op jit(solution)/shard_map/reduce_scatter | solution.py:156
  226.7 3.3 copy-start.2
  230.1 4.3 %copy-start.11 = (f32[16,4]{0,1:T(4,128)S(1)}, f32[16,4]{0,1:T(4,128)}, u32[]{:S(2)}) copy-start(f32[16,4]{0,1:T(4,128)} %param.37) | copy-start | bytes 772
  230.1 36.3 %copy-start.6 = (bf16[16,4096]{1,0:T(8,128)(2,1)S(1)}, bf16[16,4096]{1,0:T(8,128)(2,1)}, u32[]{:S(2)}) copy-start(bf16[16,4096]{1,0:T(8,128)(2,1)} %copy-done.5) | copy-start | bytes 393220
  260.8 15.1 %all-to-all-start.3 = ((bf16[8,16,1024]{2,1,0:T(8,128)(2,1)}), bf16[8,16,1024]{2,1,0:T(8,128)(2,1)S(1)}, u32[]{:S(2)}, u32[]{:S(2)}) async-start(bf16[8,16,1024]{2,1,0:T(8,128)(2,1)} %bitcast.19), calls=%async_computation.5 | async-start | bytes 524288 | tf_op jit(solution)/shard_map/all_to_all | solution.py:141
Sparse Core Ops, SparseCore 0:
  28.5 60.0 reduce-scatter.3
  127.6 31.3 all-reduce.1
  181.1 45.6 all-gather.1
  229.1 29.8 reduce-scatter.5
  262.2 62.6 reduce-scatter.7
where the time goes:
time: 334 us; the launch traced here: 333 us
  waiting for transfers between devices  221 us (66%)
  blocking collectives  44.9 us (13%)
  matrix products  26.6 us (8%)
  starting transfers between devices  14.8 us (4%)
  between operations  13.5 us (4%)
  other arithmetic  10.4 us (3%)
    reduce_scatter x1, waiting for transfers between devices, shards(): lax.psum_scatter(jnp.concatenate([jnp.dot(row_block, matrix, preferred_el...  59.1 us
    reduce_scatter x1, waiting for transfers between devices, shards(): lax.psum_scatter(jnp.dot(row_block, dense_down, preferred_element_type=jn...  48 us
    psum x1, waiting for transfers between devices, shards(): column_total = lax.psum(column_terms, 'tp')  31.3 us
    all_gather x1, blocking collectives, shards(): lax.all_gather(attended, 'ep', axis=0, tiled=True)  30.5 us
    all_to_all x1, waiting for transfers between devices, shards(): lax.all_to_all(outgoing, 'ep', split_axis=0, concat_axis=0, tiled=True)  27.4 us
    reduce_scatter x1, waiting for transfers between devices, shards(): lax.psum_scatter(partial_rows, 'tp', scatter_dimension=1, tiled=True)  24.5 us
    all_to_all x1, blocking collectives, shards(): lax.all_to_all(normed, 'ep', split_axis=1, concat_axis=0, tiled=True)  14.4 us
    all_gather x1, waiting for transfers between devices, shards(): piece = lax.all_gather(second, 'ep', axis=0, tiled=True)  14 us
  transfers between devices with their start and end apart: 8, of which 8 were waited for; matrix products, arithmetic and copies ran while one was open for 6% of the time, Pallas kernels for 0%

commit v1 on v0

--- a/solution.py
+++ b/solution.py
@@ -105,7 +105,7 @@
         out_weight,
         preferred_element_type=jnp.float32,
     )
-    column_total = lax.psum(column_terms, "tp")
+    column_total = jnp.sum(lax.all_gather(column_terms, "tp"), axis=0)
     summed = lax.all_to_all(column_total, "ep", split_axis=0, concat_axis=1, tiled=True)
     mixed = (tokens.astype(jnp.float32) + summed).astype(jnp.bfloat16)
     second = rms_scaled(mixed, mix_gain).astype(jnp.bfloat16)

time: 334 us -> 322 us (0.964)
  waiting for transfers between devices: 221 us -> 207 us
    psum x1 -> x0, waiting for transfers between devices: 31.3 us -> none  [shards(): column_total = lax.psum(column_terms, 'tp')]
    all_gather x0 -> x1, waiting for transfers between devices: none -> 15.7 us  [shards(): column_total = jnp.sum(lax.all_gather(column_terms, 'tp'), axis=0)]
where the time goes in v1:
time: 322 us; the launch traced here: 321 us
  waiting for transfers between devices  207 us (64%)
  blocking collectives  44.9 us (14%)
  matrix products  26.6 us (8%)
  starting transfers between devices  14.8 us (5%)
  between operations  13.4 us (4%)
  other arithmetic  12.4 us (4%)
    reduce_scatter x1, waiting for transfers between devices, shards(): lax.psum_scatter(jnp.concatenate([jnp.dot(row_block, matrix, preferred_el...  59.1 us
    reduce_scatter x1, waiting for transfers between devices, shards(): lax.psum_scatter(jnp.dot(row_block, dense_down, preferred_element_type=jn...  48 us
    all_gather x1, blocking collectives, shards(): lax.all_gather(attended, 'ep', axis=0, tiled=True)  30.5 us
    all_to_all x1, waiting for transfers between devices, shards(): lax.all_to_all(outgoing, 'ep', split_axis=0, concat_axis=0, tiled=True)  29.2 us
    reduce_scatter x1, waiting for transfers between devices, shards(): lax.psum_scatter(partial_rows, 'tp', scatter_dimension=1, tiled=True)  24.5 us
    all_gather x1, waiting for transfers between devices, shards(): column_total = jnp.sum(lax.all_gather(column_terms, 'tp'), axis=0)  15.7 us
    all_to_all x1, blocking collectives, shards(): lax.all_to_all(normed, 'ep', split_axis=1, concat_axis=0, tiled=True)  14.4 us
    all_gather x1, waiting for transfers between devices, shards(): piece = lax.all_gather(second, 'ep', axis=0, tiled=True)  12.6 us
  transfers between devices with their start and end apart: 8, of which 8 were waited for; matrix products, arithmetic and copies ran while one was open for 6% of the time, Pallas kernels for 0%

profile of v1, /device:TPU:0, one launch (start us, length us, event | category | flops | bytes accessed | tf_op | source)
XLA Modules:
  0.0 320.9 jit_solution(13253524367830139938)
XLA Ops:
  6.6 1.2 fusion.48
  7.8 1.0 fusion.50
  8.9 14.4 %all_to_all.48 = bf16[16,8,512]{2,0,1:T(8,128)(2,1)S(1)} all-to-all(bf16[16,8,512]{2,0,1:T(8,128)(2,1)S(1)} %bitcast.122), channel_id=1, replica_groups=mesh['ep'=8,'tp'=4] {'ep'}, dimensions={1} | all-to-all | bytes 262144 | tf_op jit(solution)/shard_map/all_to_all | solution.py:84
  24.1 1.0 fusion.83
  25.2 1.0 fusion.82
  26.2 1.3 fusion.81
  27.5 0.9 pad_maximum_fusion
  29.4 59.1 %reduce-scatter.4.cloned.1.call-done = f32[16,648]{1,0:T(8,128)} async-done(((f32[128,648]{1,0:T(8,128)}), f32[16,648]{1,0:T(8,128)}) %reduce-scatter.4.cloned.1.call-update) | async-done | bytes 41488 | tf_op jit(solution)/shard_map/reduce_scatter | solution.py:86
  89.6 0.9 fusion.69
  90.5 3.7 %fusion.80 = (f32[16,8]{1,0:T(8,128)S(1)}, f32[16,1,8,1024]{3,2,0,1:T(8,128)S(1)}) fusion(f32[16,1024,8]{1,2,0:T(8,128)S(1)} %copy-done.3, f32[16,8]{1,0:T(8,128)S(1)} %fusion.69, bf16[16,8,64]{2,1,0:T(8,128)(2,1)S(1)} %reshape.186, bf16[16,1024,1,128]{3,1,2,0:T(8,128)(2,1)} %param.28, pred[16,1024]{1,0:T(8,128)(4,1)S(1)} %iota_compare_fusion.1), kind=kOutput, calls=%fused_computation.96 | convolution fusion | flops 17432448 | bytes 5276672 | tf_op jit(solution)/shard_map/skgd,slkd->skgl/dot_general | solution.py:31
  94.5 1.4 fusion.37
  96.0 30.5 %all_gather.12 = bf16[128,512]{1,0:T(8,128)(2,1)S(1)} all-gather(bf16[16,512]{1,0:T(8,128)(2,1)S(1)} %reshape.191), channel_id=1, replica_groups=mesh['ep'=8,'tp'=4] {'ep'}, dimensions={0}, use_global_device_ids=true | all-gather | bytes 147456 | tf_op jit(solution)/shard_map/all_gather | solution.py:104
  126.6 1.0 fusion.85
  127.7 15.7 %all-gather.6.cloned.1.call-done = f32[512,512]{1,0:T(8,128)} async-done(((f32[128,512]{1,0:T(8,128)}), f32[512,512]{1,0:T(8,128)}) %all-gather.6.cloned.1.call-update) | async-done | bytes 1048592 | tf_op jit(solution)/shard_map/all_gather | solution.py:108
  143.4 2.0 reduce_sum.70
  145.5 5.5 %all-to-all-start.1 = ((f32[8,16,512]{2,1,0:T(8,128)}), f32[8,16,512]{2,1,0:T(8,128)S(1)}, u32[]{:S(2)}, u32[]{:S(2)}) async-start(f32[8,16,512]{2,1,0:T(8,128)} %bitcast.13), calls=%async_computation.2 | async-start | bytes 524288 | tf_op jit(solution)/shard_map/all_to_all | solution.py:109
  151.6 8.7 %all-to-all-done.1 = f32[8,16,512]{2,1,0:T(8,128)S(1)} async-done(((f32[8,16,512]{2,1,0:T(8,128)}), f32[8,16,512]{2,1,0:T(8,128)S(1)}, u32[]{:S(2)}, u32[]{:S(2)}) %all-to-all-start.1) | async-done | bytes 262176 | tf_op jit(solution)/shard_map/all_to_all | solution.py:109
  160.7 1.5 convolution_convert_fusion
  162.1 3.6 %all-to-all-start.2 = ((bf16[8,16,4096]{2,1,0:T(8,128)(2,1)}), bf16[8,16,4096]{2,1,0:T(8,128)(2,1)S(1)}, u32[]{:S(2)}, u32[]{:S(2)}) async-start(bf16[8,16,4096]{2,1,0:T(8,128)(2,1)} %bitcast.113), calls=%async_computation.3 | async-start | bytes 2097152 | tf_op jit(solution)/shard_map/all_to_all | solution.py:132
  166.5 29.2 %all-to-all-done.2 = bf16[8,16,4096]{2,1,0:T(8,128)(2,1)S(1)} async-done(((bf16[8,16,4096]{2,1,0:T(8,128)(2,1)}), bf16[8,16,4096]{2,1,0:T(8,128)(2,1)S(1)}, u32[]{:S(2)}, u32[]{:S(2)}) %all-to-all-start.2) | async-done | bytes 1048608 | tf_op jit(solution)/shard_map/all_to_all | solution.py:132
  195.6 2.0 fusion.10
  197.7 4.3 %fusion.6 = f32[128,4096]{1,0:T(8,128)} fusion(bf16[1,256,4096]{2,1,0:T(8,128)(2,1)S(1)} %copy-done, bf16[128,4096]{1,0:T(8,128)(2,1)S(1)} %bitcast.111, bf16[1,4096,256]{2,1,0:T(8,128)(2,1)} %param.34, f32[128,256]{1,0:T(8,128)S(1)} %fusion.10), kind=kOutput, calls=%fused_computation.8 | convolution fusion | flops 537067520 | bytes 7471104 | tf_op jit(solution)/shard_map/dot_general | solution.py:138
  202.0 12.6 %all-gather.4.cloned.1.call-done = bf16[128,4096]{1,0:T(8,128)(2,1)} async-done(((bf16[16,4096]{1,0:T(8,128)(2,1)}), bf16[128,4096]{1,0:T(8,128)(2,1)}) %all-gather.4.cloned.1.call-update) | async-done | bytes 1048592 | tf_op jit(solution)/shard_map/all_gather | solution.py:150
  214.7 3.3 %fusion.86 = f32[128,512]{1,0:T(8,128)S(1)} fusion(bf16[128,4096]{1,0:T(8,128)(2,1)} %all-gather.4.cloned.1.call-done, bf16[4096,512]{1,0:T(8,128)(2,1)} %param.38), kind=kOutput, calls=%fused_computation.102 | convolution fusion | flops 536870912 | bytes 5505024 | tf_op jit(solution)/shard_map/dot_general | solution.py:152
  218.0 4.3 %fusion.25 = f32[128,1024]{1,0:T(8,128)} fusion(bf16[512,1024]{1,0:T(8,128)(2,1)} %param.40, bf16[128,4096]{1,0:T(8,128)(2,1)S(1)} %copy-done.2, bf16[4096,512]{1,0:T(8,128)(2,1)} %param.39, f32[128,512]{1,0:T(8,128)S(1)} %fusion.86), kind=kOutput, calls=%fused_computation.20 | convolution fusion | flops 671481856 | bytes 7077888 | tf_op jit(solution)/shard_map/dot_general | solution.py:157
  222.5 24.5 %reduce-scatter.6.cloned.1.call-done = f32[128,1024]{1,0:T(8,128)} async-done(((f32[128,4096]{1,0:T(8,128)}), f32[128,1024]{1,0:T(8,128)}) %reduce-scatter.6.cloned.1.call-update) | async-done | bytes 524304 | tf_op jit(solution)/shard_map/reduce_scatter | solution.py:139
  247.0 1.8 convert_element_type.82
  248.8 5.5 %all-to-all-start.3 = ((bf16[8,16,1024]{2,1,0:T(8,128)(2,1)}), bf16[8,16,1024]{2,1,0:T(8,128)(2,1)S(1)}, u32[]{:S(2)}, u32[]{:S(2)}) async-start(bf16[8,16,1024]{2,1,0:T(8,128)(2,1)} %bitcast.20), calls=%async_computation.5 | async-start | bytes 524288 | tf_op jit(solution)/shard_map/all_to_all | solution.py:141
  254.3 0.9 fusion.43
  255.2 8.6 %all-to-all-done.3 = bf16[8,16,1024]{2,1,0:T(8,128)(2,1)S(1)} async-done(((bf16[8,16,1024]{2,1,0:T(8,128)(2,1)}), bf16[8,16,1024]{2,1,0:T(8,128)(2,1)S(1)}, u32[]{:S(2)}, u32[]{:S(2)}) %all-to-all-start.3) | async-done | bytes 262176 | tf_op jit(solution)/shard_map/all_to_all | solution.py:141
  264.9 48.0 %reduce-scatter.8.cloned.1.call-done = f32[16,1024]{1,0:T(8,128)} async-done(((f32[128,1024]{1,0:T(8,128)}), f32[16,1024]{1,0:T(8,128)}) %reduce-scatter.8.cloned.1.call-update) | async-done | bytes 65552 | tf_op jit(solution)/shard_map/reduce_scatter | solution.py:156
  312.8 1.5 add_convert_fusion
  (74 shorter events, 6.6 us)
Async XLA Ops:
  6.5 191.2 %copy-start = (bf16[1,256,4096]{2,1,0:T(8,128)(2,1)S(1)}, bf16[1,256,4096]{2,1,0:T(8,128)(2,1)}, u32[]{:S(2)}) copy-start(bf16[1,256,4096]{2,1,0:T(8,128)(2,1)} %param.35) | copy-start | bytes 6291460
  6.5 22.8 %copy-start.12 = (s32[16]{0:T(128)S(1)}, s32[16]{0:T(128)}, u32[]{:S(2)}) copy-start(s32[16]{0:T(128)} %param.30) | copy-start | bytes 196
  6.5 22.6 %copy-start.3 = (f32[16,1024,8]{1,2,0:T(8,128)S(1)}, f32[16,1024,8]{1,2,0:T(8,128)}, u32[]{:S(2)}) copy-start(f32[16,1024,8]{1,2,0:T(8,128)} %param.29) | copy-start | bytes 1572868
  6.5 83.1 %copy-start.13 = (f32[8]{0:T(128)S(1)}, f32[8]{0:T(128)}, u32[]{:S(2)}) copy-start(f32[8]{0:T(128)} %param.27) | copy-start | bytes 100
  6.5 82.0 %reduce-scatter.4.cloned.1.call-start = ((), (), s32[]{:S(2)}) async-start(), calls=%async_computation.7 | async-start | bytes 442368 | tf_op jit(solution)/shard_map/reduce_scatter | solution.py:86
  28.3 115.1 %all-gather.6.cloned.1.call-start = ((), (), s32[]{:S(2)}) async-start(), calls=%async_computation.11 | async-start | bytes 1310720 | tf_op jit(solution)/shard_map/all_gather | solution.py:108
  89.5 5.0 %copy-start.1 = (bf16[16,1024,1,128]{3,1,2,0:T(8,128)(2,1)S(1)}, bf16[16,1024,1,128]{3,1,2,0:T(8,128)(2,1)}, u32[]{:S(2)}) copy-start(bf16[16,1024,1,128]{3,1,2,0:T(8,128)(2,1)} %param.28) | copy-start | bytes 12582916
  94.2 32.3 %copy-start.8 = (bf16[512,512]{1,0:T(8,128)(2,1)S(1)}, bf16[512,512]{1,0:T(8,128)(2,1)}, u32[]{:S(2)}) copy-start(bf16[512,512]{1,0:T(8,128)(2,1)} %param.31) | copy-start | bytes 1572868
  94.2 33.3 %copy-start.10 = (s32[16,4]{0,1:T(4,128)S(1)}, s32[16,4]{0,1:T(4,128)}, u32[]{:S(2)}) copy-start(s32[16,4]{0,1:T(4,128)} %param.36) | copy-start | bytes 772
  94.5 65.8 %copy-start.4 = (bf16[16,4096]{1,0:T(8,128)(2,1)S(1)}, bf16[16,4096]{1,0:T(8,128)(2,1)}, u32[]{:S(2)}) copy-start(bf16[16,4096]{1,0:T(8,128)(2,1)} %param.21) | copy-start | bytes 393220
  94.5 66.0 %copy-start.9 = (f32[4096]{0:T(1024)S(1)}, f32[4096]{0:T(1024)}, u32[]{:S(2)}) copy-start(f32[4096]{0:T(1024)} %param.32) | copy-start | bytes 49156
  145.5 14.8 %all-to-all-start.1 = ((f32[8,16,512]{2,1,0:T(8,128)}), f32[8,16,512]{2,1,0:T(8,128)S(1)}, u32[]{:S(2)}, u32[]{:S(2)}) async-start(f32[8,16,512]{2,1,0:T(8,128)} %bitcast.13), calls=%async_computation.2 | async-start | bytes 524288 | tf_op jit(solution)/shard_map/all_to_all | solution.py:109
  160.5 1.6 copy-start.7
  160.6 5.1 %copy-start.5 = (bf16[16,4096]{1,0:T(8,128)(2,1)}, bf16[16,4096]{1,0:T(8,128)(2,1)S(1)}, u32[]{:S(2)}) copy-start(bf16[16,4096]{1,0:T(8,128)(2,1)S(1)} %fusion.47) | copy-start | bytes 393220
  162.1 33.5 %all-to-all-start.2 = ((bf16[8,16,4096]{2,1,0:T(8,128)(2,1)}), bf16[8,16,4096]{2,1,0:T(8,128)(2,1)S(1)}, u32[]{:S(2)}, u32[]{:S(2)}) async-start(bf16[8,16,4096]{2,1,0:T(8,128)(2,1)} %bitcast.113), calls=%async_computation.3 | async-start | bytes 2097152 | tf_op jit(solution)/shard_map/all_to_all | solution.py:132
  165.7 49.0 %all-gather.4.cloned.1.call-start = ((), (), s32[]{:S(2)}) async-start(), calls=%async_computation.9 | async-start | bytes 1179648 | tf_op jit(solution)/shard_map/all_gather | solution.py:150
  166.4 80.5 %reduce-scatter.6.cloned.1.call-start = ((), (), s32[]{:S(2)}) async-start(), calls=%async_computation.8 | async-start | bytes 2621440 | tf_op jit(solution)/shard_map/reduce_scatter | solution.py:139
  202.0 110.9 %reduce-scatter.8.cloned.1.call-start = ((), (), s32[]{:S(2)}) async-start(), calls=%async_computation.10 | async-start | bytes 589824 | tf_op jit(solution)/shard_map/reduce_scatter | solution.py:156
  214.7 3.3 %copy-start.2 = (bf16[128,4096]{1,0:T(8,128)(2,1)S(1)}, bf16[128,4096]{1,0:T(8,128)(2,1)}, u32[]{:S(2)}) copy-start(bf16[128,4096]{1,0:T(8,128)(2,1)} %all-gather.4.cloned.1.call-done) | copy-start | bytes 3145732
  218.0 4.3 %copy-start.11 = (f32[16,4]{0,1:T(4,128)S(1)}, f32[16,4]{0,1:T(4,128)}, u32[]{:S(2)}) copy-start(f32[16,4]{0,1:T(4,128)} %param.37) | copy-start | bytes 772
  218.0 36.3 %copy-start.6 = (bf16[16,4096]{1,0:T(8,128)(2,1)S(1)}, bf16[16,4096]{1,0:T(8,128)(2,1)}, u32[]{:S(2)}) copy-start(bf16[16,4096]{1,0:T(8,128)(2,1)} %copy-done.5) | copy-start | bytes 393220
  248.8 15.1 %all-to-all-start.3 = ((bf16[8,16,1024]{2,1,0:T(8,128)(2,1)}), bf16[8,16,1024]{2,1,0:T(8,128)(2,1)S(1)}, u32[]{:S(2)}, u32[]{:S(2)}) async-start(bf16[8,16,1024]{2,1,0:T(8,128)(2,1)} %bitcast.20), calls=%async_computation.5 | async-start | bytes 524288 | tf_op jit(solution)/shard_map/all_to_all | solution.py:141
Sparse Core Ops, SparseCore 0:
  28.5 60.0 reduce-scatter.3
  127.7 15.7 all-gather.5
  168.6 45.9 all-gather.3
  217.0 29.8 reduce-scatter.5
  250.2 62.6 reduce-scatter.7
